TPU v7x, 32 devices: a whole 2x2x4 slice. The times are simulated.
32 devices in a mesh: fs: 8 (over z, y), tp: 4 (over x, core).
Axes of the slice: x: 2, y: 2, z: 4, core: 2. Of those that a mesh axis runs over, the one named last changes fastest.
Arguments:
- inputs: bfloat16 [2048, 2048], P('fs', 'tp'), may hold values from -6 to 6
- cotangent: bfloat16 [2048, 2048], P('fs', 'tp'), may hold values from -8 to 8
- gate_weight: bfloat16 [2048, 5632], P('fs', 'tp'), may hold values from -0.125 to 0.125
- up_weight: bfloat16 [2048, 5632], P('fs', 'tp'), may hold values from -0.125 to 0.125
- down_weight: bfloat16 [5632, 2048], P('tp', 'fs'), may hold values from -0.078125 to 0.078125
Outputs:
- grad_inputs: bfloat16 [2048, 2048], P('fs', 'tp')
- grad_gate: float32 [2048, 5632], P('fs', 'tp')
- grad_up: float32 [2048, 5632], P('fs', 'tp')
- grad_down: float32 [5632, 2048], P('tp', 'fs')
All inputs are finite; a program needn't handle non-finite values.
Results may differ from a plain program's by a relative error of at most 0.015.
Values may be sent and summed in bfloat16 or wider, within the bound.
A program may use at most 64 MiB of HBM per device.

v0:
```python
import jax
import jax.numpy as jnp
from jax import lax
from jax.sharding import PartitionSpec as P


def contract_rows(left, right):
    return lax.dot_general(
        left, right, (((0,), (0,)), ((), ())), preferred_element_type=jnp.float32
    )


def contract_cols(left, right):
    return lax.dot_general(
        left, right, (((1,), (1,)), ((), ())), preferred_element_type=jnp.float32
    )


def per_device(inputs, cotangent, gate_weight, up_weight, down_weight):
    whole_inputs, whole_cotangent = (
        lax.all_gather(inputs, "tp", axis=1, tiled=True),
        lax.all_gather(cotangent, "tp", axis=1, tiled=True),
    )
    gate_whole, up_whole = (
        lax.all_gather(gate_weight, "fs", axis=0, tiled=True),
        lax.all_gather(up_weight, "fs", axis=0, tiled=True),
    )
    gate_pre = jnp.dot(whole_inputs, gate_whole, preferred_element_type=jnp.float32)
    up_pre = jnp.dot(whole_inputs, up_whole, preferred_element_type=jnp.float32)
    gate_sig = jax.nn.sigmoid(gate_pre)
    gate_act = gate_pre * gate_sig
    hidden = (gate_act * up_pre).astype(jnp.bfloat16)
    grad_hidden = contract_cols(
        whole_cotangent, lax.all_gather(down_weight, "fs", axis=1, tiled=True)
    )
    grad_gate_pre = (grad_hidden * up_pre * gate_sig * (1.0 + gate_pre * (1.0 - gate_sig))).astype(
        jnp.bfloat16
    )
    grad_up_pre = (grad_hidden * gate_act).astype(jnp.bfloat16)
    pre_grads = jnp.concatenate([grad_gate_pre, grad_up_pre], axis=1)
    width = gate_weight.shape[1]
    partial_sum = contract_cols(grad_gate_pre, gate_whole) + contract_cols(grad_up_pre, up_whole)
    grad_inputs = lax.psum_scatter(
        partial_sum.astype(jnp.bfloat16), "tp", scatter_dimension=1, tiled=True
    )
    expand = lax.psum_scatter(
        contract_rows(whole_inputs, pre_grads).astype(jnp.bfloat16),
        "fs",
        scatter_dimension=0,
        tiled=True,
    ).astype(jnp.float32)
    down = lax.psum_scatter(
        contract_rows(whole_cotangent, hidden).astype(jnp.bfloat16),
        "fs",
        scatter_dimension=0,
        tiled=True,
    ).astype(jnp.float32)
    grad_gate = expand[:, :width]
    grad_up = expand[:, width:]
    grad_down = down.T
    return (grad_inputs, grad_gate, grad_up, grad_down)


def solution(mesh):
    return jax.shard_map(
        per_device,
        mesh=mesh,
        in_specs=(P("fs", "tp"), P("fs", "tp"), P("fs", "tp"), P("fs", "tp"), P("tp", "fs")),
        out_specs=(P("fs", "tp"), P("fs", "tp"), P("fs", "tp"), P("tp", "fs")),
        check_vma=False,
    )
```

profile of v0, /device:TPU:0, one launch (start us, length us, event | category | flops | bytes accessed | tf_op | source)
XLA Modules:
  0.0 670.5 jit_solution(8997837980882983968)
XLA Ops:
  7.2 0.0 all-gather.10.cloned.1.call-start
  7.2 0.7 all-gather.10.cloned.1.call-update
  7.9 0.0 all-gather.12.cloned.1.call-start
  7.9 0.7 all-gather.12.cloned.1.call-update
  8.6 0.0 all-gather.14.cloned.1.call-start
  8.7 0.7 all-gather.14.cloned.1.call-update
  9.4 0.0 all-gather.6.cloned.1.call-start
  9.4 0.5 all-gather.6.cloned.1.call-update
  10.0 0.0 all-gather.8.cloned.1.call-start
  10.0 0.5 all-gather.8.cloned.1.call-update
  10.5 0.0 reduce-scatter.8.cloned.1.call-start
  10.6 18.4 %all-gather.10.cloned.1.call-done = bf16[256,2048]{1,0:T(8,128)(2,1)} async-done(((bf16[256,512]{1,0:T(8,128)(2,1)}), bf16[256,2048]{1,0:T(8,128)(2,1)}) %all-gather.10.cloned.1.call-update) | async-done | bytes 1048592 | tf_op jit(solution)/shard_map/all_gather | solution.py:21
  29.0 0.0 copy-start
  29.0 94.5 %all-gather.12.cloned.1.call-done = bf16[2048,1408]{1,0:T(8,128)(2,1)} async-done(((bf16[256,1408]{1,0:T(8,128)(2,1)}), bf16[2048,1408]{1,0:T(8,128)(2,1)}) %all-gather.12.cloned.1.call-update) | async-done | bytes 5767184 | tf_op jit(solution)/shard_map/all_gather | solution.py:26
  123.5 4.8 fusion.10
  128.3 0.0 copy-start.2
  128.3 87.9 %all-gather.14.cloned.1.call-done = bf16[2048,1408]{1,0:T(8,128)(2,1)} async-done(((bf16[256,1408]{1,0:T(8,128)(2,1)}), bf16[2048,1408]{1,0:T(8,128)(2,1)}) %all-gather.14.cloned.1.call-update) | async-done | bytes 5767184 | tf_op jit(solution)/shard_map/all_gather | solution.py:25
  216.2 0.0 copy-done
  216.2 5.5 fusion.11
  221.8 10.8 %all-gather.6.cloned.1.call-done = bf16[256,2048]{1,0:T(8,128)(2,1)} async-done(((bf16[256,512]{1,0:T(8,128)(2,1)}), bf16[256,2048]{1,0:T(8,128)(2,1)}) %all-gather.6.cloned.1.call-update) | async-done | bytes 1048592 | tf_op jit(solution)/shard_map/all_gather | solution.py:22
  232.6 0.0 copy-done.2
  232.6 5.9 fusion
  238.5 0.0 copy-start.1
  238.5 0.0 reduce-scatter.8.cloned.1.call-update
  238.6 0.0 reduce-scatter.6.cloned.1.call-start
  238.6 89.1 %all-gather.8.cloned.1.call-done = bf16[1408,2048]{1,0:T(8,128)(2,1)} async-done(((bf16[1408,256]{1,0:T(8,128)(2,1)}), bf16[1408,2048]{1,0:T(8,128)(2,1)}) %all-gather.8.cloned.1.call-update) | async-done | bytes 5767184 | tf_op jit(solution)/shard_map/all_gather | solution.py:34
  327.7 0.0 copy-done.1
  327.7 5.6 multiply_convert_fusion.1
  333.3 6.1 convert_bitcast_fusion
  339.4 0.0 reduce-scatter.6.cloned.1.call-update
  339.4 0.2 reduce-scatter.4.cloned.1.call-start
  339.6 4.5 fusion.12
  344.1 5.5 fusion.1
  349.6 0.0 reduce-scatter.4.cloned.1.call-update
  349.6 90.8 %reduce-scatter.8.cloned.1.call-done = bf16[256,1408]{0,1:T(8,128)(2,1)} async-done(((bf16[2048,1408]{0,1:T(8,128)(2,1)}), bf16[256,1408]{0,1:T(8,128)(2,1)}) %reduce-scatter.8.cloned.1.call-update) | async-done | bytes 720912 | tf_op jit(solution)/shard_map/reduce_scatter | solution.py:52
  440.4 2.3 convert_bitcast_fusion.1
  442.8 193.9 %reduce-scatter.6.cloned.1.call-done = bf16[256,2816]{0,1:T(8,128)(2,1)} async-done(((bf16[2048,2816]{0,1:T(8,128)(2,1)}), bf16[256,2816]{0,1:T(8,128)(2,1)}) %reduce-scatter.6.cloned.1.call-update) | async-done | bytes 1441808 | tf_op jit(solution)/shard_map/reduce_scatter | solution.py:46
  636.7 1.5 fusion.9
  638.2 1.5 copy.10
  639.8 1.5 copy.9
  641.3 22.4 %reduce-scatter.4.cloned.1.call-done = bf16[256,512]{1,0:T(8,128)(2,1)} async-done(((bf16[256,2048]{1,0:T(8,128)(2,1)}), bf16[256,512]{1,0:T(8,128)(2,1)}) %reduce-scatter.4.cloned.1.call-update) | async-done | bytes 262160 | tf_op jit(solution)/shard_map/reduce_scatter | solution.py:43
Async XLA Ops:
  7.2 21.8 %all-gather.10.cloned.1.call-start = ((), (), s32[]{:S(2)}) async-start(), calls=%async_computation.5 | async-start | bytes 1310720 | tf_op jit(solution)/shard_map/all_gather | solution.py:21
  7.9 115.6 %all-gather.12.cloned.1.call-start = ((), (), s32[]{:S(2)}) async-start(), calls=%async_computation.6 | async-start | bytes 6488064 | tf_op jit(solution)/shard_map/all_gather | solution.py:26
  8.6 207.6 %all-gather.14.cloned.1.call-start = ((), (), s32[]{:S(2)}) async-start(), calls=%async_computation.7 | async-start | bytes 6488064 | tf_op jit(solution)/shard_map/all_gather | solution.py:25
  9.4 223.2 %all-gather.6.cloned.1.call-start = ((), (), s32[]{:S(2)}) async-start(), calls=%async_computation.3 | async-start | bytes 1310720 | tf_op jit(solution)/shard_map/all_gather | solution.py:22
  10.0 317.7 %all-gather.8.cloned.1.call-start = ((), (), s32[]{:S(2)}) async-start(), calls=%async_computation.4 | async-start | bytes 6488064 | tf_op jit(solution)/shard_map/all_gather | solution.py:34
  10.5 429.9 %reduce-scatter.8.cloned.1.call-start = ((), (), s32[]{:S(2)}) async-start(), calls=%async_computation.10 | async-start | bytes 6488064 | tf_op jit(solution)/shard_map/reduce_scatter | solution.py:52
  29.0 187.2 %copy-start = (bf16[256,2048]{1,0:T(8,128)(2,1)S(1)}, bf16[256,2048]{1,0:T(8,128)(2,1)}, u32[]{:S(2)}) copy-start(bf16[256,2048]{1,0:T(8,128)(2,1)} %all-gather.10.cloned.1.call-done) | copy-start | bytes 3145732
  128.3 104.3 %copy-start.2 = (f32[256,1408]{1,0:T(8,128)}, f32[256,1408]{1,0:T(8,128)S(1)}, u32[]{:S(2)}) copy-start(f32[256,1408]{1,0:T(8,128)S(1)} %fusion.10) | copy-start | bytes 4325380
  238.5 89.1 %copy-start.1 = (bf16[256,2048]{1,0:T(8,128)(2,1)S(1)}, bf16[256,2048]{1,0:T(8,128)(2,1)}, u32[]{:S(2)}) copy-start(bf16[256,2048]{1,0:T(8,128)(2,1)} %all-gather.6.cloned.1.call-done) | copy-start | bytes 3145732
  238.6 398.1 %reduce-scatter.6.cloned.1.call-start = ((), (), s32[]{:S(2)}) async-start(), calls=%async_computation.9 | async-start | bytes 12976128 | tf_op jit(solution)/shard_map/reduce_scatter | solution.py:46
  339.4 324.3 %reduce-scatter.4.cloned.1.call-start = ((), (), s32[]{:S(2)}) async-start(), calls=%async_computation.8 | async-start | bytes 1310720 | tf_op jit(solution)/shard_map/reduce_scatter | solution.py:43
Sparse Core Ops, SparseCore 0:
  9.5 19.4 all-gather.9
  31.2 92.2 all-gather.11
  125.7 90.4 all-gather.13
  217.6 14.9 all-gather.5
  234.5 93.1 all-gather.7
  331.2 109.2 reduce-scatter.7
  444.0 192.6 reduce-scatter.5
  639.8 23.8 reduce-scatter.3
where the time goes:
time: 671 us
  waiting for transfers between devices  611 us (91%)
  matrix products  37.9 us (6%)
  between operations  14.2 us (2%)
    reduce_scatter x1, waiting for transfers between devices, per_device(): lax.psum_scatter(contract_rows(whole_inputs, pre_grads).astype(jnp.bfloat...  194 us
    all_gather x1, waiting for transfers between devices, per_device(): lax.all_gather(up_weight, 'fs', axis=0, tiled=True)  94.5 us
    reduce_scatter x1, waiting for transfers between devices, per_device(): lax.psum_scatter(contract_rows(whole_cotangent, hidden).astype(jnp.bfloat...  90.8 us
    all_gather x1, waiting for transfers between devices, per_device(): lax.all_gather(down_weight, 'fs', axis=1, tiled=True)  89.1 us
    all_gather x1, waiting for transfers between devices, per_device(): lax.all_gather(gate_weight, 'fs', axis=0, tiled=True)  87.9 us
    reduce_scatter x1, waiting for transfers between devices, per_device(): lax.psum_scatter(partial_sum.astype(jnp.bfloat16), 'tp', scatter_dimensio...  22.4 us
    all_gather x1, waiting for transfers between devices, per_device(): lax.all_gather(inputs, 'tp', axis=1, tiled=True)  18.4 us
    dot_general x3, matrix products, contract_cols(): lax.dot_general(left, right, (((1,), (1,)), ((), ())), preferred_element_...  15.6 us
  transfers between devices with their start and end apart: 8, of which 8 were waited for; matrix products, arithmetic and copies ran while one was open for 7% of the time, Pallas kernels for 0%

commit v1 on v0

--- a/solution.py
+++ b/solution.py
@@ -2,6 +2,11 @@
 import jax.numpy as jnp
 from jax import lax
 from jax.sharding import PartitionSpec as P
+
+
+def swapped_in(array, axis, dim):
+    sent = jnp.stack([array] * lax.axis_size(axis))
+    return jnp.concatenate(lax.all_to_all(sent, axis, 0, 0), axis=dim)
 
 
 def contract_rows(left, right):
@@ -30,9 +35,7 @@
     gate_sig = jax.nn.sigmoid(gate_pre)
     gate_act = gate_pre * gate_sig
     hidden = (gate_act * up_pre).astype(jnp.bfloat16)
-    grad_hidden = contract_cols(
-        whole_cotangent, lax.all_gather(down_weight, "fs", axis=1, tiled=True)
-    )
+    grad_hidden = contract_cols(whole_cotangent, swapped_in(down_weight, "fs", 1))
     grad_gate_pre = (grad_hidden * up_pre * gate_sig * (1.0 + gate_pre * (1.0 - gate_sig))).astype(
         jnp.bfloat16
     )

time: 671 us -> 668 us (level)
  waiting for transfers between devices: 611 us -> 597 us
  starting transfers between devices: 0.49 us -> 7.76 us
    all_gather x1 -> x0, waiting for transfers between devices: 89.1 us -> none  [per_device(): lax.all_gather(down_weight, 'fs', axis=1, tiled=True)]
    all_gather x1, waiting for transfers between devices: 94.5 us -> 182 us  [per_device(): lax.all_gather(up_weight, 'fs', axis=0, tiled=True)]
    all_gather x1, waiting for transfers between devices: 18.4 us -> 8.37 us  [per_device(): lax.all_gather(inputs, 'tp', axis=1, tiled=True)]
    all_to_all x0 -> x1, starting transfers between devices: none -> 7.31 us  [swapped_in(): return jnp.concatenate(lax.all_to_all(sent, axis, 0, 0), axis=dim)]
  transfers between devices with their start and end apart: 8 -> 8, of which waited for: 8 -> 7; matrix products, arithmetic and copies ran while one was open for 7% -> 7% of each run, Pallas kernels for 0% -> 0%
where the time goes in v1:
time: 668 us
  waiting for transfers between devices  597 us (89%)
  matrix products  37.7 us (6%)
  between operations  14.2 us (2%)
  local copies, waits for them, and re-layouts  9.07 us (1%)
  starting transfers between devices  7.76 us (1%)
    reduce_scatter x1, waiting for transfers between devices, per_device(): lax.psum_scatter(contract_rows(whole_inputs, pre_grads).astype(jnp.bfloat...  194 us
    all_gather x1, waiting for transfers between devices, per_device(): lax.all_gather(up_weight, 'fs', axis=0, tiled=True)  182 us
    all_gather x1, waiting for transfers between devices, per_device(): lax.all_gather(gate_weight, 'fs', axis=0, tiled=True)  88.6 us
    reduce_scatter x1, waiting for transfers between devices, per_device(): lax.psum_scatter(contract_rows(whole_cotangent, hidden).astype(jnp.bfloat...  88.2 us
    reduce_scatter x1, waiting for transfers between devices, per_device(): lax.psum_scatter(partial_sum.astype(jnp.bfloat16), 'tp', scatter_dimensio...  22.4 us
    dot_general x3, matrix products, contract_cols(): lax.dot_general(left, right, (((1,), (1,)), ((), ())), preferred_element_...  15.4 us
  transfers between devices with their start and end apart: 8, of which 7 were waited for; matrix products, arithmetic and copies ran while one was open for 7% of the time, Pallas kernels for 0%

profile of v1, /device:TPU:0, one launch (start us, length us, event | category | flops | bytes accessed | tf_op | source)
XLA Modules:
  0.0 667.7 jit_solution(977462011852424877)
XLA Ops:
  7.2 0.0 copy-start.1
  7.2 0.0 all-gather.7.cloned.1.call-start
  7.2 0.7 all-gather.7.cloned.1.call-update
  7.9 0.0 all-gather.9.cloned.1.call-start
  8.0 0.7 all-gather.9.cloned.1.call-update
  8.7 0.0 all-gather.11.cloned.1.call-start
  8.7 0.7 all-gather.11.cloned.1.call-update
  9.4 0.0 all-gather.5.cloned.1.call-start
  9.4 0.5 all-gather.5.cloned.1.call-update
  10.0 0.0 copy-done.1
  10.0 0.3 copy.11
  10.3 2.9 stack.2
  13.3 7.3 %all-to-all-start = ((bf16[8,1408,256]{1,2,0:T(8,128)(2,1)}), bf16[8,1408,256]{1,2,0:T(8,128)(2,1)}, u32[]{:S(2)}, u32[]{:S(2)}) async-start(bf16[8,1408,256]{1,2,0:T(8,128)(2,1)} %stack.2), calls=%async_computation | async-start | bytes 11534336 | tf_op jit(solution)/shard_map/all_to_all | solution.py:9
  20.6 0.0 reduce-scatter.8.cloned.1.call-start
  20.6 8.4 %all-gather.7.cloned.1.call-done = bf16[256,2048]{1,0:T(8,128)(2,1)} async-done(((bf16[256,512]{1,0:T(8,128)(2,1)}), bf16[256,2048]{1,0:T(8,128)(2,1)}) %all-gather.7.cloned.1.call-update) | async-done | bytes 1048592 | tf_op jit(solution)/shard_map/all_gather | solution.py:26
  29.0 0.0 copy-start
  29.0 181.9 %all-gather.9.cloned.1.call-done = bf16[2048,1408]{1,0:T(8,128)(2,1)} async-done(((bf16[256,1408]{1,0:T(8,128)(2,1)}), bf16[2048,1408]{1,0:T(8,128)(2,1)}) %all-gather.9.cloned.1.call-update) | async-done | bytes 5767184 | tf_op jit(solution)/shard_map/all_gather | solution.py:31
  210.9 4.8 fusion.10
  215.7 0.0 copy-start.3
  215.7 88.6 %all-gather.11.cloned.1.call-done = bf16[2048,1408]{1,0:T(8,128)(2,1)} async-done(((bf16[256,1408]{1,0:T(8,128)(2,1)}), bf16[2048,1408]{1,0:T(8,128)(2,1)}) %all-gather.11.cloned.1.call-update) | async-done | bytes 5767184 | tf_op jit(solution)/shard_map/all_gather | solution.py:30
  304.3 0.0 copy-done
  304.3 5.5 fusion.11
  309.8 10.8 %all-gather.5.cloned.1.call-done = bf16[256,2048]{1,0:T(8,128)(2,1)} async-done(((bf16[256,512]{1,0:T(8,128)(2,1)}), bf16[256,2048]{1,0:T(8,128)(2,1)}) %all-gather.5.cloned.1.call-update) | async-done | bytes 1048592 | tf_op jit(solution)/shard_map/all_gather | solution.py:27
  320.6 0.0 copy-done.3
  320.6 5.9 fusion
  326.6 0.0 copy-start.2
  326.6 0.0 reduce-scatter.8.cloned.1.call-update
  326.6 0.0 reduce-scatter.6.cloned.1.call-start
  326.6 0.0 all-to-all-done
  326.6 1.1 copy-done.2
  327.8 5.4 multiply_convert_fusion.1
  333.2 6.1 convert_bitcast_fusion
  339.3 0.0 reduce-scatter.6.cloned.1.call-update
  339.3 0.2 reduce-scatter.4.cloned.1.call-start
  339.6 4.5 fusion.12
  344.1 5.5 fusion.1
  349.6 0.0 reduce-scatter.4.cloned.1.call-update
  349.6 88.2 %reduce-scatter.8.cloned.1.call-done = bf16[256,1408]{0,1:T(8,128)(2,1)} async-done(((bf16[2048,1408]{0,1:T(8,128)(2,1)}), bf16[256,1408]{0,1:T(8,128)(2,1)}) %reduce-scatter.8.cloned.1.call-update) | async-done | bytes 720912 | tf_op jit(solution)/shard_map/reduce_scatter | solution.py:55
  437.8 2.3 convert_bitcast_fusion.1
  440.1 193.7 %reduce-scatter.6.cloned.1.call-done = bf16[256,2816]{0,1:T(8,128)(2,1)} async-done(((bf16[2048,2816]{0,1:T(8,128)(2,1)}), bf16[256,2816]{0,1:T(8,128)(2,1)}) %reduce-scatter.6.cloned.1.call-update) | async-done | bytes 1441808 | tf_op jit(solution)/shard_map/reduce_scatter | solution.py:49
  633.8 1.5 fusion.9
  635.4 1.5 copy.13
  636.9 1.5 copy.12
  638.4 22.4 %reduce-scatter.4.cloned.1.call-done = bf16[256,512]{1,0:T(8,128)(2,1)} async-done(((bf16[256,2048]{1,0:T(8,128)(2,1)}), bf16[256,512]{1,0:T(8,128)(2,1)}) %reduce-scatter.4.cloned.1.call-update) | async-done | bytes 262160 | tf_op jit(solution)/shard_map/reduce_scatter | solution.py:46
Async XLA Ops:
  7.2 2.8 copy-start.1
  7.2 21.8 %all-gather.7.cloned.1.call-start = ((), (), s32[]{:S(2)}) async-start(), calls=%async_computation.5 | async-start | bytes 1310720 | tf_op jit(solution)/shard_map/all_gather | solution.py:26
  7.9 203.0 %all-gather.9.cloned.1.call-start = ((), (), s32[]{:S(2)}) async-start(), calls=%async_computation.6 | async-start | bytes 6488064 | tf_op jit(solution)/shard_map/all_gather | solution.py:31
  8.7 295.6 %all-gather.11.cloned.1.call-start = ((), (), s32[]{:S(2)}) async-start(), calls=%async_computation.7 | async-start | bytes 6488064 | tf_op jit(solution)/shard_map/all_gather | solution.py:30
  9.4 311.2 %all-gather.5.cloned.1.call-start = ((), (), s32[]{:S(2)}) async-start(), calls=%async_computation.4 | async-start | bytes 1310720 | tf_op jit(solution)/shard_map/all_gather | solution.py:27
  13.3 313.4 %all-to-all-start = ((bf16[8,1408,256]{1,2,0:T(8,128)(2,1)}), bf16[8,1408,256]{1,2,0:T(8,128)(2,1)}, u32[]{:S(2)}, u32[]{:S(2)}) async-start(bf16[8,1408,256]{1,2,0:T(8,128)(2,1)} %stack.2), calls=%async_computation | async-start | bytes 11534336 | tf_op jit(solution)/shard_map/all_to_all | solution.py:9
  20.6 417.2 %reduce-scatter.8.cloned.1.call-start = ((), (), s32[]{:S(2)}) async-start(), calls=%async_computation.10 | async-start | bytes 6488064 | tf_op jit(solution)/shard_map/reduce_scatter | solution.py:55
  29.0 275.3 %copy-start = (bf16[256,2048]{1,0:T(8,128)(2,1)S(1)}, bf16[256,2048]{1,0:T(8,128)(2,1)}, u32[]{:S(2)}) copy-start(bf16[256,2048]{1,0:T(8,128)(2,1)} %all-gather.7.cloned.1.call-done) | copy-start | bytes 3145732
  215.7 105.0 %copy-start.3 = (f32[256,1408]{1,0:T(8,128)}, f32[256,1408]{1,0:T(8,128)S(1)}, u32[]{:S(2)}) copy-start(f32[256,1408]{1,0:T(8,128)S(1)} %fusion.10) | copy-start | bytes 4325380
  326.6 1.2 copy-start.2
  326.6 307.2 %reduce-scatter.6.cloned.1.call-start = ((), (), s32[]{:S(2)}) async-start(), calls=%async_computation.9 | async-start | bytes 12976128 | tf_op jit(solution)/shard_map/reduce_scatter | solution.py:49
  339.3 321.5 %reduce-scatter.4.cloned.1.call-start = ((), (), s32[]{:S(2)}) async-start(), calls=%async_computation.8 | async-start | bytes 1310720 | tf_op jit(solution)/shard_map/reduce_scatter | solution.py:46
Sparse Core Ops, SparseCore 0:
  9.5 19.4 all-gather.6
  31.2 179.6 all-gather.8
  213.1 91.1 all-gather.10
  305.7 14.9 all-gather.4
  326.7 111.0 reduce-scatter.7
  441.3 192.4 reduce-scatter.5
  636.9 23.8 reduce-scatter.3
